TPU v7x, 32 devices: a whole 2x2x4 slice. The times are simulated.
32 devices in a mesh: sp: 4 (over z), tp: 4 (over y, x), dp: 2 (over core).
Axes of the slice: x: 2, y: 2, z: 4, core: 2. Of those that a mesh axis runs over, the one named last changes fastest.
Arguments:
- latent: bfloat16 [2, 1024, 2048], P('dp', 'sp'), may hold values from -1.5 to 1.5
- condition: bfloat16 [2, 2048], P('dp', 'sp'), may hold values from -6 to 6
- context: bfloat16 [2, 1024, 2048], P('dp', 'sp'), may hold values from -6 to 6
- context_code: bfloat16 [2048], P('sp'), may hold values from -6 to 6
- shift_weight: bfloat16 [2048, 2048], P('sp', 'tp'), may hold values from -0.125 to 0.125
- scale_weight: bfloat16 [2048, 2048], P('sp', 'tp'), may hold values from -0.125 to 0.125
- gate_weight: bfloat16 [2048, 2048], P('sp', 'tp'), may hold values from -0.125 to 0.125
- norm_gain: float32 [2048], replicated, may hold values from 0.1 to 1.9
- query_weight: bfloat16 [2048, 1024], P(None, 'tp'), may hold values from -0.125 to 0.125
- key_weight: bfloat16 [2048, 256], P(None, 'tp'), may hold values from -0.125 to 0.125
- value_weight: bfloat16 [2048, 256], P(None, 'tp'), may hold values from -0.125 to 0.125
- output_weight: bfloat16 [1024, 2048], P('tp'), may hold values from -0.75 to 0.75
- query_gain: float32 [64], replicated, may hold values from 1 to 5.5
- key_gain: float32 [64], replicated, may hold values from 1 to 5.5
- context_bias: float32 [16], P('tp'), may hold values from 0.5 to 2
Outputs:
- updated: bfloat16 [2, 1024, 2048], P('dp', 'sp')
All inputs are finite; a program needn't handle non-finite values.
Results may differ from a plain program's by a relative error of at most 0.01405.
The roundings to bfloat16 on the way count: a program that leaves them out, or rounds other values in their place, can miss the bound.
Values may be sent and summed in bfloat16 or wider, within the bound.
A program may use at most 64 MiB of HBM per device.

v0:
```python
import math

import jax
import jax.numpy as jnp
from jax import lax
from jax.sharding import PartitionSpec as P

GRID_W = 64


norm_eps = 1e-06
rope_base = 10000.0


def rotary_tables(position, grid_width, head_dim):
    grid_row = (position // grid_width).astype(jnp.float32)
    grid_col = (position % grid_width).astype(jnp.float32)
    quarter = head_dim // 4
    inverse = rope_base ** (-jnp.arange(quarter, dtype=jnp.float32) / quarter)
    angles = jnp.concatenate([grid_row[:, None] * inverse, grid_col[:, None] * inverse], axis=-1)
    return (jnp.cos(angles), jnp.sin(angles))


def head_norm(values, gain_row):
    return (
        values * lax.rsqrt(jnp.mean(values * values, axis=-1, keepdims=True) + norm_eps) * gain_row
    )


def rotate(values, cosine, sine_part):
    half_dim = values.shape[-1] // 2
    first_half = values[..., :half_dim]
    second_half = values[..., half_dim:]
    cos_rows = cosine[:, None, :]
    sin_rows = sine_part[:, None, :]
    return jnp.concatenate(
        [
            first_half * cos_rows - second_half * sin_rows,
            second_half * cos_rows + first_half * sin_rows,
        ],
        axis=-1,
    )


def modulated(tokens, gain_row, shift_row, scale_row):
    floats = tokens.astype(jnp.float32)
    normal = floats * lax.rsqrt(jnp.mean(floats * floats, axis=-1, keepdims=True) + norm_eps)
    return (normal * gain_row * (1.0 + scale_row) + shift_row).astype(jnp.bfloat16)


def on_device(
    latent,
    condition,
    context,
    context_code,
    shift_weight,
    scale_weight,
    gate_weight,
    norm_gain,
    query_weight,
    key_weight,
    value_weight,
    output_weight,
    query_gain,
    key_gain,
    context_bias,
):
    head_dim = query_gain.shape[0]
    tp_size = lax.axis_size("tp")
    activated = jax.nn.silu(condition[0].astype(jnp.float32)).astype(jnp.bfloat16)
    context_act = jax.nn.silu(context_code.astype(jnp.float32)).astype(jnp.bfloat16)
    partial_mod = jnp.stack(
        [
            jnp.dot(activated, shift_weight, preferred_element_type=jnp.float32),
            jnp.dot(activated, scale_weight, preferred_element_type=jnp.float32),
            jnp.dot(activated, gate_weight, preferred_element_type=jnp.float32),
            jnp.dot(context_act, shift_weight, preferred_element_type=jnp.float32),
            jnp.dot(context_act, scale_weight, preferred_element_type=jnp.float32),
        ]
    )
    summed = lax.psum(partial_mod, "sp")
    vectors = lax.all_gather(summed, "tp", axis=1, tiled=True)
    normed = modulated(latent[0], norm_gain, vectors[0], vectors[1])
    query_cols = query_weight.shape[1]
    key_cols = key_weight.shape[1]
    projected = jnp.concatenate(
        [
            jnp.dot(normed, query_weight, preferred_element_type=jnp.float32),
            jnp.dot(normed, key_weight, preferred_element_type=jnp.float32),
            jnp.dot(normed, value_weight, preferred_element_type=jnp.float32),
        ],
        axis=1,
    )
    seq_rows = projected.shape[0]
    position = lax.axis_index("sp") * seq_rows + jnp.arange(seq_rows, dtype=jnp.int32)
    cosine, sine_part = rotary_tables(position, GRID_W, head_dim)
    group_size = query_cols // head_dim
    queries = projected[:, :query_cols].reshape(seq_rows, group_size, head_dim)
    queries = rotate(head_norm(queries, query_gain), cosine, sine_part).astype(jnp.bfloat16)
    latent_keys = projected[:, query_cols : query_cols + key_cols].reshape(seq_rows, 1, head_dim)
    latent_keys = rotate(head_norm(latent_keys, key_gain), cosine, sine_part).astype(jnp.bfloat16)
    latent_values = projected[:, query_cols + key_cols :].astype(jnp.bfloat16)
    key_value = jnp.concatenate([latent_keys.reshape(seq_rows, head_dim), latent_values], axis=1)
    context_normed = modulated(context[0], norm_gain, vectors[3], vectors[4])
    context_keys = head_norm(
        jnp.dot(context_normed, key_weight, preferred_element_type=jnp.float32), key_gain
    )
    context_values = jnp.dot(context_normed, value_weight, preferred_element_type=jnp.float32)
    context_kv = lax.all_gather(
        jnp.concatenate(
            [context_keys.astype(jnp.bfloat16), context_values.astype(jnp.bfloat16)], axis=1
        ),
        "sp",
        axis=0,
        tiled=True,
    )
    score_scale = head_dim ** (-0.5)
    query_rows = queries.transpose(1, 0, 2).reshape(group_size * seq_rows, head_dim)
    bias_rows = jnp.repeat(context_bias, seq_rows)
    context_scores = jnp.dot(
        query_rows, context_kv[:, :head_dim].T, preferred_element_type=jnp.float32
    )
    context_scores = context_scores * score_scale + bias_rows[:, None]
    first_max = context_scores.max(axis=1)
    context_exp = jnp.exp(context_scores - first_max[:, None])
    start_state = (
        first_max,
        context_exp.sum(axis=1),
        jnp.dot(
            context_exp.astype(jnp.bfloat16),
            context_kv[:, head_dim:],
            preferred_element_type=jnp.float32,
        ),
    )
    arrived = lax.all_gather(key_value, "sp", axis=0, tiled=True)
    arrived_rows = arrived.shape[0]
    block_rows = math.gcd(arrived_rows, 1024)
    blocks = arrived.reshape(arrived_rows // block_rows, block_rows, 2 * head_dim)

    def absorb_block(state_now, pair_block):
        old_max, old_total, old_accum = state_now
        scores = (
            jnp.dot(query_rows, pair_block[:, :head_dim].T, preferred_element_type=jnp.float32)
            * score_scale
        )
        new_max = jnp.maximum(old_max, scores.max(axis=1))
        factor = jnp.exp(old_max - new_max)
        weights = jnp.exp(scores - new_max[:, None])
        new_accum = old_accum * factor[:, None] + jnp.dot(
            weights.astype(jnp.bfloat16),
            pair_block[:, head_dim:],
            preferred_element_type=jnp.float32,
        )
        return ((new_max, old_total * factor + weights.sum(axis=1), new_accum), None)

    final_state, unused = lax.scan(absorb_block, start_state, blocks)
    row_max, totals, accum = final_state
    attended = (accum / totals[:, None]).astype(jnp.bfloat16)
    attended = (
        attended.reshape(group_size, seq_rows, head_dim)
        .transpose(1, 0, 2)
        .reshape(seq_rows, query_cols)
    )
    own_rows = seq_rows // tp_size
    mixed = lax.psum_scatter(
        jnp.dot(attended, output_weight, preferred_element_type=jnp.float32).astype(jnp.bfloat16),
        "tp",
        scatter_dimension=0,
        tiled=True,
    ).astype(jnp.float32)
    own_latent = lax.dynamic_slice_in_dim(latent[0], lax.axis_index("tp") * own_rows, own_rows, 0)
    updated = (own_latent.astype(jnp.float32) + vectors[2] * mixed).astype(jnp.bfloat16)
    whole = lax.all_gather(updated, "tp", axis=0, tiled=True)
    return whole[None]


def solution(mesh):
    return jax.shard_map(
        on_device,
        mesh=mesh,
        in_specs=(
            P("dp", "sp", None),
            P("dp", "sp"),
            P("dp", "sp", None),
            P("sp"),
            P("sp", "tp"),
            P("sp", "tp"),
            P("sp", "tp"),
            P(),
            P(None, "tp"),
            P(None, "tp"),
            P(None, "tp"),
            P("tp", None),
            P(),
            P(),
            P("tp"),
        ),
        out_specs=P("dp", "sp", None),
        check_vma=False,
    )
```

profile of v0, /device:TPU:0, one launch (start us, length us, event | category | flops | bytes accessed | tf_op | source)
XLA Modules:
  0.0 148.6 jit_solution(14240642526981248333)
XLA Ops:
  6.6 0.8 fusion.67
  7.4 1.3 fusion.79
  8.7 1.2 fusion.78
  9.9 0.7 convert_element_type.122
  10.7 1.2 fusion.76
  11.9 1.2 fusion.75
  13.1 0.3 fusion.16
  13.5 0.3 fusion.7
  13.8 0.2 fusion.77
  14.0 20.5 %psum.7 = f32[5,512]{1,0:T(8,128)S(1)} all-reduce(f32[5,512]{1,0:T(8,128)S(1)} %stack.23), channel_id=1, replica_groups=mesh['sp'=4,'tp'=4,'dp'=2] {'sp'}, use_global_device_ids=true, to_apply=%region_0.1 | all-reduce | flops 2560 | bytes 20480 | tf_op jit(solution)/shard_map/psum | solution.py:81
  34.5 8.4 %all_gather.12 = f32[5,2048]{1,0:T(8,128)S(1)} all-gather(f32[5,512]{1,0:T(8,128)S(1)} %psum.7), channel_id=1, replica_groups=mesh['sp'=4,'tp'=4,'dp'=2] {'tp'}, dimensions={1}, use_global_device_ids=true | all-gather | bytes 51200 | tf_op jit(solution)/shard_map/all_gather | solution.py:82
  42.9 0.0 copy-done.9
  42.9 0.0 copy-done.12
  42.9 0.6 convolution_convert_fusion.2
  43.5 0.0 copy-start.10
  43.6 0.6 multiply_reduce_fusion.3
  44.2 0.3 copy-done.10
  44.5 0.6 convolution_convert_fusion.1
  45.1 0.0 copy-start.8
  45.1 0.0 copy-start.6
  45.1 0.0 copy-start.3
  45.2 0.6 multiply_reduce_fusion.2
  45.8 0.1 broadcast_bitcast_fusion
  45.9 0.1 multiply_bitcast_fusion
  46.0 15.3 %all_gather.13 = bf16[1024,128]{0,1:T(8,128)(2,1)} all-gather(bf16[256,128]{0,1:T(8,128)(2,1)S(1)} %pad_maximum_fusion), channel_id=1, replica_groups=mesh['sp'=4,'tp'=4,'dp'=2] {'sp'}, dimensions={0}, use_global_device_ids=true | all-gather | bytes 327680 | tf_op jit(solution)/shard_map/all_gather | solution.py:109
  61.3 0.1 fusion.63
  61.4 0.1 fusion.61
  61.5 13.8 %all_gather.14 = bf16[1024,128]{0,1:T(8,128)(2,1)S(1)} all-gather(bf16[256,128]{0,1:T(8,128)(2,1)S(1)} %pad_maximum_fusion.1), channel_id=1, replica_groups=mesh['sp'=4,'tp'=4,'dp'=2] {'sp'}, dimensions={0}, use_global_device_ids=true | all-gather | bytes 327680 | tf_op jit(solution)/shard_map/all_gather | solution.py:135
  75.3 1.4 copy.17
  76.7 1.9 %multiply_reduce_fusion.1 = (f32[256,4]{0,1:T(4,128)S(1)}, f32[256,4,64]{0,2,1:T(8,128)S(1)}) fusion(bf16[4,64,2048]{2,1,0:T(8,128)(2,1)} %bitcast.98, bf16[1,256,2048]{2,1,0:T(8,128)(2,1)S(1)} %copy-done.1, f32[2048]{0:T(1024)S(1)} %bitcast.107, f32[2048]{0:T(1024)S(1)} %bitcast.110, f32[2048]{0:T(1024)S(1)} %copy-done.12, f32[256]{0:T(256)S(1)} %add_rsqrt_fusion.4), kind=kOutput, calls=%fused_computation.47 | convolution fusion | flops 271711232 | bytes 2388992 | tf_op jit(solution)/shard_map/dot_general | solution.py:88
  78.7 0.1 fusion.60
  78.8 0.0 copy-done.7
  78.8 0.1 multiply_multiply_fusion
  79.0 0.8 multiply_reduce_fusion
  79.8 0.2 copy-done.4
  80.0 0.8 fusion
  80.8 0.9 fusion.3
  81.6 0.7 fusion.1
  82.4 1.0 fusion.25
  83.3 0.8 fusion.34
  84.2 1.4 convolution_convert_fusion
  85.6 0.0 reduce-scatter.2.cloned.1.call-update
  85.6 0.0 all-gather.2.cloned.1.call-start
  85.7 25.4 %reduce-scatter.2.cloned.1.call-done = bf16[64,2048]{1,0:T(8,128)(2,1)} async-done(((bf16[256,2048]{1,0:T(8,128)(2,1)}), bf16[64,2048]{1,0:T(8,128)(2,1)}) %reduce-scatter.2.cloned.1.call-update) | async-done | bytes 262160 | tf_op jit(solution)/shard_map/reduce_scatter | solution.py:165
  111.1 1.7 %fusion.44 = bf16[64,2048]{1,0:T(8,128)(2,1)} fusion(bf16[64,2048]{1,0:T(8,128)(2,1)} %reduce-scatter.2.cloned.1.call-done, f32[2048]{0:T(1024)S(1)} %bitcast.104, bf16[1,256,2048]{2,1,0:T(8,128)(2,1)S(1)} %copy-done.1, s32[]{:T(128)S(6)} %select_n.23), kind=kLoop, calls=%fused_computation.45 | loop fusion | flops 655360 | bytes 794628 | tf_op jit(solution)/shard_map/convert_element_type | solution.py:172
  112.8 0.0 all-gather.2.cloned.1.call-update
  112.8 26.7 %all-gather.2.cloned.1.call-done = bf16[256,2048]{1,0:T(8,128)(2,1)} async-done(((bf16[64,2048]{1,0:T(8,128)(2,1)}), bf16[256,2048]{1,0:T(8,128)(2,1)}) %all-gather.2.cloned.1.call-update) | async-done | bytes 1048592 | tf_op jit(solution)/shard_map/all_gather | solution.py:173
  139.5 2.3 %copy.26 = bf16[1,256,2048]{2,1,0:T(8,128)(2,1)} copy(bf16[1,256,2048]{2,1,0:T(8,128)(2,1)} %bitcast.97) | data formatting | bytes 2097152
  (38 shorter events, 0.3 us)
Async XLA Ops:
  6.5 77.6 %copy-start = (bf16[256,2048]{1,0:T(8,128)(2,1)S(1)}, bf16[256,2048]{1,0:T(8,128)(2,1)}, u32[]{:S(2)}) copy-start(bf16[256,2048]{1,0:T(8,128)(2,1)} %param.26) | copy-start | bytes 3145732
  6.5 6.6 %copy-start.2 = (bf16[1,256,2048]{2,1,0:T(8,128)(2,1)S(1)}, bf16[1,256,2048]{2,1,0:T(8,128)(2,1)}, u32[]{:S(2)}) copy-start(bf16[1,256,2048]{2,1,0:T(8,128)(2,1)} %param.17) | copy-start | bytes 3145732
  6.5 6.9 %copy-start.1 = (bf16[1,256,2048]{2,1,0:T(8,128)(2,1)S(1)}, bf16[1,256,2048]{2,1,0:T(8,128)(2,1)}, u32[]{:S(2)}) copy-start(bf16[1,256,2048]{2,1,0:T(8,128)(2,1)} %param.15) | copy-start | bytes 3145732
  6.5 104.5 %reduce-scatter.2.cloned.1.call-start = ((), (), s32[]{:S(2)}) async-start(), calls=%async_computation.1 | async-start | bytes 1310720 | tf_op jit(solution)/shard_map/reduce_scatter | solution.py:165
  7.4 6.3 %copy-start.5 = (bf16[512,512]{1,0:T(8,128)(2,1)S(1)}, bf16[512,512]{1,0:T(8,128)(2,1)}, u32[]{:S(2)}) copy-start(bf16[512,512]{1,0:T(8,128)(2,1)} %param.21) | copy-start | bytes 1572868
  9.9 33.0 %copy-start.9 = (bf16[2048,64]{0,1:T(8,128)(2,1)S(1)}, bf16[2048,64]{0,1:T(8,128)(2,1)}, u32[]{:S(2)}) copy-start(bf16[2048,64]{0,1:T(8,128)(2,1)} %param.25) | copy-start | bytes 786436
  9.9 33.0 %copy-start.12 = (f32[2048]{0:T(1024)S(1)}, f32[2048]{0:T(1024)}, u32[]{:S(2)}) copy-start(f32[2048]{0:T(1024)} %param.22) | copy-start | bytes 24580
  34.5 9.1 %copy-start.11 = (bf16[2048,64]{0,1:T(8,128)(2,1)S(1)}, bf16[2048,64]{0,1:T(8,128)(2,1)}, u32[]{:S(2)}) copy-start(bf16[2048,64]{0,1:T(8,128)(2,1)} %param.24) | copy-start | bytes 786436
  43.5 1.0 copy-start.10
  45.1 0.7 copy-start.8
  45.1 0.8 copy-start.6
  45.1 30.2 %copy-start.3 = (bf16[2048,256]{1,0:T(8,128)(2,1)S(1)}, bf16[2048,256]{1,0:T(8,128)(2,1)}, u32[]{:S(2)}) copy-start(bf16[2048,256]{1,0:T(8,128)(2,1)} %param.23) | copy-start | bytes 3145732
  76.7 2.1 %copy-start.7 = (f32[64]{0:T(128)S(1)}, f32[64]{0:T(128)}, u32[]{:S(2)}) copy-start(f32[64]{0:T(128)} %param.27) | copy-start | bytes 772
  79.0 1.0 copy-start.4
  85.6 53.8 %all-gather.2.cloned.1.call-start = ((), (), s32[]{:S(2)}) async-start(), calls=%async_computation.2 | async-start | bytes 1310720 | tf_op jit(solution)/shard_map/all_gather | solution.py:173
Sparse Core Ops, SparseCore 0:
  85.8 25.2 reduce-scatter.1
  113.0 26.4 all-gather.1
where the time goes:
time: 149 us
  blocking collectives  57.9 us (39%)
  waiting for transfers between devices  52.1 us (35%)
  matrix products  14.3 us (10%)
  between operations  13.7 us (9%)
  other arithmetic  6.16 us (4%)
  local copies, waits for them, and re-layouts  4.4 us (3%)
    all_gather x1, waiting for transfers between devices, on_device(): whole = lax.all_gather(updated, 'tp', axis=0, tiled=True)  26.7 us
    reduce_scatter x1, waiting for transfers between devices, on_device(): lax.psum_scatter(jnp.dot(attended, output_weight, preferred_element_type=...  25.4 us
    psum x1, blocking collectives, on_device(): summed = lax.psum(partial_mod, 'sp')  20.5 us
    all_gather x1, blocking collectives, on_device(): lax.all_gather(jnp.concatenate([context_keys.astype(jnp.bfloat16), contex...  15.3 us
    all_gather x1, blocking collectives, on_device(): arrived = lax.all_gather(key_value, 'sp', axis=0, tiled=True)  13.8 us
    all_gather x1, blocking collectives, on_device(): vectors = lax.all_gather(summed, 'tp', axis=1, tiled=True)  8.36 us
    unnamed x30, local copies, waits for them, and re-layouts  4.33 us
  transfers between devices with their start and end apart: 2, of which 2 were waited for; matrix products, arithmetic and copies ran while one was open for 0% of the time, Pallas kernels for 0%

commit v1 on v0

v1 whole, which is shorter than its diff:
```python
import functools
import math

import jax
import jax.numpy as jnp
from jax import lax
from jax.experimental import pallas as pl
from jax.experimental.pallas import tpu as pltpu
from jax.sharding import PartitionSpec as P

GRID_W = 64
norm_eps = 1e-06
rope_base = 10000.0
F32 = jnp.float32
BF16 = jnp.bfloat16
LOW = -1e30


def tables(first, rows, head_dim):
    quarter = head_dim // 4
    half = head_dim // 2
    shape = (rows, head_dim)
    token = first + lax.broadcasted_iota(jnp.int32, shape, 0)
    lane = lax.broadcasted_iota(jnp.int32, shape, 1)
    pair = lane % half
    index = (pair % quarter).astype(F32)
    place = jnp.where(pair < quarter, token // GRID_W, token % GRID_W).astype(F32)
    angle = place * jnp.exp(index * (-math.log(rope_base) / quarter))
    sine = jnp.sin(angle)
    return jnp.cos(angle), jnp.where(lane < half, -sine, sine)


def head_norm(values, gain_row):
    mean = jnp.mean(values * values, axis=-1, keepdims=True)
    return values * lax.rsqrt(mean + norm_eps) * gain_row


def rotate(values, cosine, sine):
    half = values.shape[-1] // 2
    swapped = jnp.concatenate([values[:, half:], values[:, :half]], axis=1)
    return values * cosine + swapped * sine


def kernel(
    sizes,
    condition, code, gain_ref, q_gain, k_gain, bias_ref,
    latent, context, shift_w, scale_w, gate_w, wq, wk, wv, wo,
    out,
    modw, lat, ctx, wq_v, wkv, wbuf,
    vec_z, vec_t, normed, kvbuf, q_s, m_s, acc, att, mixed, cos_s, sin_s, inv_s, out_v,
    local, out_sem,
    z_send, z_recv, t_send, t_recv, kv_send, kv_recv,
    w_send, w_recv, f_send, f_recv, a_send, a_recv,
):
    n_sp, n_tp, n_dp = sizes
    sp, tp, dp = lax.axis_index("sp"), lax.axis_index("tp"), lax.axis_index("dp")
    rows, crows = lat.shape[0], ctx.shape[0]
    hd = wk.shape[0]
    qcols = wq_v.shape[1]
    heads = qcols // hd
    width = lat.shape[1]
    cols = width // n_tp
    dots = functools.partial(jnp.dot, preferred_element_type=F32)

    copies = {}
    for number, (name, src, dst) in enumerate((
        ("m0", shift_w, modw.at[0]), ("m1", scale_w, modw.at[1]), ("m2", gate_w, modw.at[2]),
        ("wk", wk, wkv.at[:hd]), ("wv", wv, wkv.at[hd:]), ("ctx", context.at[0], ctx), ("lat", latent.at[0], lat),
        ("wq", wq, wq_v), ("wo", wo, wbuf.at[tp]),
    )):
        copies[name] = pltpu.make_async_copy(src, dst, local.at[number])
        copies[name].start()

    barrier = pltpu.get_barrier_semaphore()
    for d in range(1, n_sp):
        pl.semaphore_signal(barrier, inc=1, device_id={"sp": (sp + d) % n_sp}, device_id_type=pl.DeviceIdType.MESH)
    for d in range(1, n_tp):
        pl.semaphore_signal(barrier, inc=1, device_id={"tp": tp ^ d}, device_id_type=pl.DeviceIdType.MESH)
    for d in range(1, n_dp):
        pl.semaphore_signal(barrier, inc=1, device_id={"dp": (dp + d) % n_dp}, device_id_type=pl.DeviceIdType.MESH)

    def remote(src, dst, s, r, **where):
        return pltpu.make_async_remote_copy(
            src_ref=src, dst_ref=dst, send_sem=s, recv_sem=r,
            device_id=where, device_id_type=pl.DeviceIdType.MESH)

    row8 = lax.broadcasted_iota(jnp.int32, (8, condition.shape[1]), 0)
    own_code = condition[...].astype(F32)
    shared_code = code[...].astype(F32)
    both = jnp.where(row8 == 0, own_code, jnp.where(row8 == 1, shared_code, 0.0))
    both = (both / (1.0 + jnp.exp(-both))).astype(BF16)
    pieces = []
    for k in range(3):
        copies[f"m{k}"].wait()
        pieces.append(dots(both, modw[k])[:2])
    vec_z[sp] = jnp.concatenate(pieces + [jnp.zeros_like(pieces[0])], axis=0)

    pl.semaphore_wait(barrier, n_sp + n_tp + n_dp - 3)
    z_copies = []
    for d in range(1, n_sp):
        copy = remote(vec_z.at[sp], vec_z.at[sp], z_send.at[d], z_recv.at[d], sp=(sp + d) % n_sp)
        copy.start()
        z_copies.append(copy)

    share = wo.shape[0] // n_dp
    piece = share // 2

    def span(core, part):
        return pl.ds(core * share + part * piece, piece)

    near = [d for d in (1, 2) if d < n_tp]
    waiting = []

    def send_weights(part):
        for d in near:
            copy = remote(wo.at[span(dp, part)], wbuf.at[tp, span(dp, part)],
                          w_send.at[d, part], w_recv.at[d, part], tp=tp ^ d)
            copy.start()
            waiting.append(copy)

    def got_weights(d, part):
        ref = wbuf.at[tp ^ d, span(dp, part)]
        remote(ref, ref, w_send.at[d, part], w_recv.at[d, part], tp=tp ^ d).wait_recv()
        if n_tp == 4 and (d, part) in ((2, 0), (1, 1)):
            copy = remote(ref, ref, w_send.at[3, part], w_recv.at[3, part], tp=tp ^ (3 - d))
            copy.start()
            waiting.append(copy)
        for e in range(1, n_dp):
            copy = remote(ref, ref, f_send.at[d, part, e], f_recv.at[d, part, e], dp=(dp + e) % n_dp)
            copy.start()
            waiting.append(copy)

    send_weights(0)

    cosine, sine = tables(sp * rows, rows, hd)
    cos_s[...] = cosine
    sin_s[...] = sine
    copies["ctx"].wait()
    floats = ctx[...].astype(F32)
    inv_c = lax.rsqrt(jnp.mean(floats * floats, axis=-1, keepdims=True) + norm_eps)
    copies["lat"].wait()
    floats = lat[...].astype(F32)
    inv_s[...] = lax.rsqrt(jnp.mean(floats * floats, axis=-1, keepdims=True) + norm_eps)

    for copy in z_copies:
        copy.wait()
    total = vec_z[0]
    for k in range(1, n_sp):
        total = total + vec_z[k]
    vec_t[tp] = total
    for d in range(1, n_tp):
        copy = remote(vec_t.at[tp], vec_t.at[tp], t_send.at[d], t_recv.at[d], tp=tp ^ d)
        copy.start()
        waiting.append(copy)
    send_weights(1)
    for d in range(1, n_tp):
        remote(vec_t.at[tp ^ d], vec_t.at[tp ^ d], t_send.at[d], t_recv.at[d], tp=tp ^ d).wait_recv()

    def modulate(tokens, inverse, which):
        for t in range(n_tp):
            part = slice(t * cols, (t + 1) * cols)
            factor = gain_ref[:, part] * (1.0 + vec_t[t, 2 + which:3 + which, :])
            shift = vec_t[t, which:which + 1, :]
            normed[:tokens.shape[0], part] = (tokens[:, part].astype(F32) * inverse * factor + shift).astype(BF16)

    lanes = 2 * hd

    def kv_copy(block, target, way, part):
        area = pl.ds(0, crows) if part == 0 else pl.ds(crows, rows)
        ref = kvbuf.at[block, area]
        return remote(ref, ref, kv_send.at[way, part, block], kv_recv.at[part, block], sp=target)

    def send_own(part):
        @pl.when(sp + 1 < n_sp)
        def _():
            kv_copy(sp, sp + 1, 0, part).start()

        @pl.when(sp > 0)
        def _():
            kv_copy(sp, sp - 1, 1, part).start()

    dims = (((1,), (1,)), ((), ()))
    modulate(ctx, inv_c, 1)
    copies["wk"].wait()
    copies["wv"].wait()
    kv = lax.dot_general(normed[:crows], wkv[...], dims, preferred_element_type=F32)
    kvbuf[sp, :crows] = jnp.concatenate([head_norm(kv[:, :hd], k_gain[...]), kv[:, hd:]], axis=1).astype(BF16)
    send_own(0)

    modulate(lat, inv_s[...], 0)
    kv = lax.dot_general(normed[:rows], wkv[...], dims, preferred_element_type=F32)
    keys = rotate(head_norm(kv[:, :hd], k_gain[...]), cos_s[...], sin_s[...])
    kvbuf[sp, crows:] = jnp.concatenate([keys, kv[:, hd:]], axis=1).astype(BF16)
    send_own(1)

    copies["wq"].wait()
    queries = dots(normed[:rows], wq_v[...])
    for h in range(heads):
        one = rotate(head_norm(queries[:, h * hd:(h + 1) * hd], q_gain[...]), cos_s[...], sin_s[...])
        q_s[h] = (one * hd ** -0.5).astype(BF16)
    m_s[...] = jnp.full_like(m_s, LOW)
    acc[...] = jnp.zeros_like(acc)

    for d in near:
        got_weights(d, 0)

    def absorb(block):
        @pl.loop(0, heads)
        def _(h):
            bias = bias_ref[h]
            query = q_s[h]
            s_c = lax.dot_general(query, kvbuf[block, :crows, :hd], dims, preferred_element_type=F32)
            s_l = lax.dot_general(query, kvbuf[block, crows:, :hd], dims, preferred_element_type=F32)
            old = m_s[h]
            new = jnp.maximum(old, jnp.maximum(
                s_c.max(axis=1, keepdims=True) + bias, s_l.max(axis=1, keepdims=True)))
            m_s[h] = new
            p_c = jnp.exp(s_c - (new - bias)).astype(BF16)
            p_l = jnp.exp(s_l - new).astype(BF16)

            def values(pairs):
                lane = lax.broadcasted_iota(jnp.int32, pairs.shape, 1)
                return jnp.where(lane < hd, jnp.ones_like(pairs), pairs)

            acc[h] = (acc[h] * jnp.exp(old - new)
                      + dots(p_c, values(kvbuf[block, :crows]))
                      + dots(p_l, values(kvbuf[block, crows:])))

    absorb(sp)
    for d in near:
        got_weights(d, 1)

    @pl.loop(1, n_sp)
    def _(s):
        for part in range(2):
            @pl.when(sp - s >= 0)
            def _():
                kv_copy(sp - s, sp, 0, part).wait_recv()

                @pl.when(sp + 1 < n_sp)
                def _():
                    kv_copy(sp - s, sp + 1, 0, part).start()

            @pl.when(sp + s < n_sp)
            def _():
                kv_copy(sp + s, sp, 1, part).wait_recv()

                @pl.when(sp > 0)
                def _():
                    kv_copy(sp + s, sp - 1, 1, part).start()

        @pl.when(sp - s >= 0)
        def _():
            absorb(sp - s)

        @pl.when(sp + s < n_sp)
        def _():
            absorb(sp + s)

    if n_tp == 4:
        for part in range(2):
            got_weights(3, part)

    for g in range(heads // 2):
        pair = []
        for h in (2 * g, 2 * g + 1):
            whole = acc[h]
            pair.append(whole[:, hd:] / whole[:, :hd])
        att[tp, g] = jnp.concatenate(pair, axis=1).astype(BF16)
        for d in range(1, n_tp):
            copy = remote(att.at[tp, g], att.at[tp, g], a_send.at[d, g], a_recv.at[d, g], tp=tp ^ d)
            copy.start()
            waiting.append(copy)

    copies["wo"].wait()
    step = cols

    def project(group):
        left = jnp.concatenate([att[group, g] for g in range(heads // 2)], axis=1)
        return lambda part: dots(left, wbuf[group, :, part]).astype(BF16).astype(F32)

    def arrive(d):
        for core in range(1, n_dp):
            source = (dp + n_dp - core) % n_dp
            for part in range(2):
                ref = wbuf.at[tp ^ d, span(source, part)]
                remote(ref, ref, f_send.at[d, part, core], f_recv.at[d, part, core], dp=source).wait_recv()
        for g in range(heads // 2):
            ref = att.at[tp ^ d, g]
            remote(ref, ref, a_send.at[d, g], a_recv.at[d, g], tp=tp ^ d).wait_recv()
        return project(tp ^ d)

    for d in range(n_tp):
        term = project(tp) if d == 0 else arrive(d)
        for t in range(n_tp):
            part = slice(t * step, (t + 1) * step)
            value = term(part)
            if d > 0:
                value = mixed[:, part] + value
            if d < n_tp - 1:
                mixed[:, part] = value
            else:
                gate = vec_t[t, 4:5, :]
                out_v[:, part] = (lat[:, part].astype(F32) + gate * value).astype(BF16)
    back = pltpu.make_async_copy(out_v, out.at[0], out_sem)
    back.start()

    for copy in waiting:
        copy.wait_send()

    @pl.loop(0, n_sp)
    def _(b):
        for part in range(2):
            @pl.when((b <= sp) & (sp + 1 < n_sp))
            def _():
                kv_copy(b, sp, 0, part).wait_send()

            @pl.when((b >= sp) & (sp > 0))
            def _():
                kv_copy(b, sp, 1, part).wait_send()
    back.wait()


def on_device(
    sizes, latent, condition, context, context_code, shift_weight, scale_weight, gate_weight,
    norm_gain, query_weight, key_weight, value_weight, output_weight, query_gain, key_gain,
    context_bias,
):
    n_sp, n_tp, n_dp = sizes
    rows, width = latent.shape[1:]
    crows = context.shape[1]
    hd = query_gain.shape[0]
    qcols = query_weight.shape[1]
    heads = qcols // hd
    deep, cols = shift_weight.shape
    vmem = pl.BlockSpec(memory_space=pltpu.VMEM)
    smem = pl.BlockSpec(memory_space=pltpu.SMEM)
    hbm = pl.BlockSpec(memory_space=pl.ANY)
    dma = pltpu.SemaphoreType.DMA
    most = max(rows, crows)
    scratch = [
        pltpu.VMEM((3, deep, cols), BF16),
        pltpu.VMEM((rows, width), BF16),
        pltpu.VMEM((crows, width), BF16),
        pltpu.VMEM((width, qcols), BF16),
        pltpu.VMEM((2 * hd, width), BF16),
        pltpu.VMEM((n_tp,) + output_weight.shape, BF16),
        pltpu.VMEM((n_sp, 8, cols), F32),
        pltpu.VMEM((n_tp, 8, cols), F32),
        pltpu.VMEM((most, width), BF16),
        pltpu.VMEM((n_sp, crows + rows, 2 * hd), BF16),
        pltpu.VMEM((heads, rows, hd), BF16),
        pltpu.VMEM((heads, rows, 1), F32),
        pltpu.VMEM((heads, rows, 2 * hd), F32),
        pltpu.VMEM((n_tp, heads // 2, rows, 2 * hd), BF16),
        pltpu.VMEM((rows, width), F32),
        pltpu.VMEM((rows, hd), F32),
        pltpu.VMEM((rows, hd), F32),
        pltpu.VMEM((rows, 1), F32),
        pltpu.VMEM((rows, width), BF16),
        dma((9,)), dma,
        dma((n_sp,)), dma((n_sp,)), dma((n_tp,)), dma((n_tp,)),
        dma((2, 2, n_sp)), dma((2, n_sp)),
        dma((n_tp, 2)), dma((n_tp, 2)), dma((n_tp, 2, n_dp)), dma((n_tp, 2, n_dp)),
        dma((n_tp, heads // 2)), dma((n_tp, heads // 2)),
    ]
    return pl.pallas_call(
        functools.partial(kernel, sizes),
        out_shape=jax.ShapeDtypeStruct(latent.shape, BF16),
        in_specs=[vmem] * 5 + [smem] + [hbm] * 9,
        out_specs=hbm,
        scratch_shapes=scratch,
        compiler_params=pltpu.CompilerParams(
            collective_id=0, has_side_effects=True, vmem_limit_bytes=60 * 1024 * 1024),
    )(
        condition, context_code[None], norm_gain[None], query_gain[None], key_gain[None],
        context_bias, latent, context, shift_weight, scale_weight, gate_weight, query_weight,
        key_weight.T, value_weight.T, output_weight,
    )


def solution(mesh):
    sizes = tuple(mesh.shape[axis] for axis in ("sp", "tp", "dp"))
    return jax.shard_map(
        functools.partial(on_device, sizes),
        mesh=mesh,
        in_specs=(
            P("dp", "sp", None),
            P("dp", "sp"),
            P("dp", "sp", None),
            P("sp"),
            P("sp", "tp"),
            P("sp", "tp"),
            P("sp", "tp"),
            P(),
            P(None, "tp"),
            P(None, "tp"),
            P(None, "tp"),
            P("tp", None),
            P(),
            P(),
            P("tp"),
        ),
        out_specs=P("dp", "sp", None),
        check_vma=False,
    )
```

time: 149 us -> 45.3 us (0.30)
  blocking collectives: 57.9 us -> 0 us
  waiting for transfers between devices: 52.1 us -> 0 us
  Pallas kernels: 0 us -> 41.5 us
  matrix products: 14.3 us -> 0 us
  between operations: 13.7 us -> 0.01 us
  other arithmetic: 6.16 us -> 0 us
    pallas_call x0 -> x1, Pallas kernels: none -> 41.5 us  [on_device(): pl.pallas_call(functools.partial(kernel, sizes), out_shape=jax.ShapeDtype...]
    all_gather x3 -> x0, blocking collectives: 37.4 us -> none  [the longest x1 15.3 us: on_device(): lax.all_gather(jnp.concatenate([context_keys.astype(jnp.bfloat16), contex...]
    all_gather x1 -> x0, waiting for transfers between devices: 26.7 us -> none  [on_device(): whole = lax.all_gather(updated, 'tp', axis=0, tiled=True)]
    reduce_scatter x1 -> x0, waiting for transfers between devices: 25.4 us -> none  [on_device(): lax.psum_scatter(jnp.dot(attended, output_weight, preferred_element_type=...]
    psum x1 -> x0, blocking collectives: 20.5 us -> none  [on_device(): summed = lax.psum(partial_mod, 'sp')]
    dot_general x15 -> x0, matrix products: 14.3 us -> none  [the longest x1 1.94 us: on_device(): jnp.dot(normed, query_weight, preferred_element_type=jnp.float32)]
    convert_element_type x5 -> x0, other arithmetic: 3.34 us -> none  [the longest x1 1.73 us: on_device(): (own_latent.astype(jnp.float32) + vectors[2] * mixed).astype(jnp.bfloat16)]
    reduce_sum x4 -> x0, other arithmetic: 2.17 us -> none  [the longest x1 0.86 us: on_device(): context_exp.sum(axis=1)]
  transfers between devices with their start and end apart: 2 -> 0, of which waited for: 2 -> 0; matrix products, arithmetic and copies ran while one was open for 0% -> 0% of each run, Pallas kernels for 0% -> 0%
where the time goes in v1:
time: 45.3 us; the launch traced here: 45.1 us
  Pallas kernels  41.5 us (92%)
  local copies, waits for them, and re-layouts  3.56 us (8%)
    pallas_call x1, Pallas kernels, on_device(): pl.pallas_call(functools.partial(kernel, sizes), out_shape=jax.ShapeDtype...  41.5 us
    unnamed x3, local copies, waits for them, and re-layouts  2.98 us

profile of v1, /device:TPU:0, one launch (start us, length us, event | category | flops | bytes accessed | tf_op | source)
XLA Modules:
  0.0 45.1 jit_solution(11149573567513343518)
XLA Ops:
  0.0 0.0 copy-start
  0.0 0.7 %copy-done = bf16[512]{0:T(512)(128)(2,1)S(1)} copy-done((bf16[512]{0:T(512)(128)(2,1)S(1)}, bf16[512]{0:T(512)(128)(2,1)}, u32[]{:S(2)}) %copy-start) | copy-done | bytes 1048
  0.7 0.6 %broadcast_in_dim.12.code = bf16[1,512]{1,0:T(2,128)(2,1)} reshape(bf16[512]{0:T(512)(128)(2,1)S(1)} %copy-done) | data formatting | bytes 2048 | tf_op jit(solution)/shard_map/broadcast_in_dim | solution.py:376
  1.3 41.5 %shard_map.145 = bf16[1,256,2048]{2,1,0:T(8,128)(2,1)} custom-call(bf16[1,512]{1,0:T(2,128)(2,1)} %condition.1, bf16[1,512]{1,0:T(2,128)(2,1)} %broadcast_in_dim.12.code, f32[1,2048]{1,0:T(1,128)} %bitcast.7, f32[1,64]{1,0:T(1,128)} %bitcast.8, f32[1,64]{1,0:T(1,128)} %bitcast.9, f32[4]{0:T(128)} %bias_ref.1, bf16[1,256,2048]{2,1,0:T(8,128)(2,1)} %latent.1, ...), custom_call_target="tpu_custom_call" | custom-call | tf_op jit(solution)/shard_map/pallas_call | solution.py:367
  42.8 2.3 %copy.17 = bf16[1,256,2048]{2,1,0:T(8,128)(2,1)} copy(bf16[1,256,2048]{2,1,0:T(8,128)(2,1)} %shard_map.145) | data formatting | bytes 2097152
Async XLA Ops:
  0.0 0.7 %copy-start = (bf16[512]{0:T(512)(128)(2,1)S(1)}, bf16[512]{0:T(512)(128)(2,1)}, u32[]{:S(2)}) copy-start(bf16[512]{0:T(512)(128)(2,1)} %param.18) | copy-start | bytes 3076

commit v2 on v1

--- a/solution.py
+++ b/solution.py
@@ -47,8 +47,8 @@
     latent, context, shift_w, scale_w, gate_w, wq, wk, wv, wo,
     out,
     modw, lat, ctx, wq_v, wkv, wbuf,
-    vec_z, vec_t, normed, kvbuf, q_s, m_s, acc, att, mixed, cos_s, sin_s, inv_s, out_v,
-    local, out_sem,
+    vec_z, vec_t, normed, kvbuf, q_s, m_s, acc, att, mixed, cos_s, sin_s, inv_s,
+    local,
     z_send, z_recv, t_send, t_recv, kv_send, kv_recv,
     w_send, w_recv, f_send, f_recv, a_send, a_recv,
 ):
@@ -86,7 +86,7 @@
 
     row8 = lax.broadcasted_iota(jnp.int32, (8, condition.shape[1]), 0)
     own_code = condition[...].astype(F32)
-    shared_code = code[...].astype(F32)
+    shared_code = code[...].astype(F32)[None]
     both = jnp.where(row8 == 0, own_code, jnp.where(row8 == 1, shared_code, 0.0))
     both = (both / (1.0 + jnp.exp(-both))).astype(BF16)
     pieces = []
@@ -301,9 +301,7 @@
                 mixed[:, part] = value
             else:
                 gate = vec_t[t, 4:5, :]
-                out_v[:, part] = (lat[:, part].astype(F32) + gate * value).astype(BF16)
-    back = pltpu.make_async_copy(out_v, out.at[0], out_sem)
-    back.start()
+                out[0, :, part] = (lat[:, part].astype(F32) + gate * value).astype(BF16)
 
     for copy in waiting:
         copy.wait_send()
@@ -318,7 +316,6 @@
             @pl.when((b >= sp) & (sp > 0))
             def _():
                 kv_copy(b, sp, 1, part).wait_send()
-    back.wait()
 
 
 def on_device(
@@ -335,7 +332,7 @@
     deep, cols = shift_weight.shape
     vmem = pl.BlockSpec(memory_space=pltpu.VMEM)
     smem = pl.BlockSpec(memory_space=pltpu.SMEM)
-    hbm = pl.BlockSpec(memory_space=pl.ANY)
+    hbm = pl.BlockSpec(memory_space=pltpu.HBM)
     dma = pltpu.SemaphoreType.DMA
     most = max(rows, crows)
     scratch = [
@@ -357,8 +354,7 @@
         pltpu.VMEM((rows, hd), F32),
         pltpu.VMEM((rows, hd), F32),
         pltpu.VMEM((rows, 1), F32),
-        pltpu.VMEM((rows, width), BF16),
-        dma((9,)), dma,
+        dma((9,)),
         dma((n_sp,)), dma((n_sp,)), dma((n_tp,)), dma((n_tp,)),
         dma((2, 2, n_sp)), dma((2, n_sp)),
         dma((n_tp, 2)), dma((n_tp, 2)), dma((n_tp, 2, n_dp)), dma((n_tp, 2, n_dp)),
@@ -368,12 +364,12 @@
         functools.partial(kernel, sizes),
         out_shape=jax.ShapeDtypeStruct(latent.shape, BF16),
         in_specs=[vmem] * 5 + [smem] + [hbm] * 9,
-        out_specs=hbm,
+        out_specs=vmem,
         scratch_shapes=scratch,
         compiler_params=pltpu.CompilerParams(
-            collective_id=0, has_side_effects=True, vmem_limit_bytes=60 * 1024 * 1024),
+            collective_id=0, has_side_effects=True, vmem_limit_bytes=36 * 1024 * 1024),
     )(
-        condition, context_code[None], norm_gain[None], query_gain[None], key_gain[None],
+        condition, context_code, norm_gain[None], query_gain[None], key_gain[None],
         context_bias, latent, context, shift_weight, scale_weight, gate_weight, query_weight,
         key_weight.T, value_weight.T, output_weight,
     )

time: 45.3 us -> 55.3 us (1.22)
  local copies, waits for them, and re-layouts: 3.56 us -> 14.2 us
  Pallas kernels: 41.5 us -> 40.5 us
    unnamed x3 -> x31, local copies, waits for them, and re-layouts: 2.98 us -> 14.2 us
    pallas_call x1, Pallas kernels: 41.5 us -> 40.5 us  [on_device(): pl.pallas_call(functools.partial(kernel, sizes), out_shape=jax.ShapeDtype...]
    broadcast_in_dim x1 -> x0, local copies, waits for them, and re-layouts: 0.58 us -> none  [on_device(): context_code[None]]
where the time goes in v2:
time: 55.3 us; the launch traced here: 54.7 us
  Pallas kernels  40.5 us (73%)
  local copies, waits for them, and re-layouts  14.2 us (26%)
    pallas_call x1, Pallas kernels, on_device(): pl.pallas_call(functools.partial(kernel, sizes), out_shape=jax.ShapeDtype...  40.5 us
    unnamed x31, local copies, waits for them, and re-layouts  14.2 us

profile of v2, /device:TPU:0, one launch (start us, length us, event | category | flops | bytes accessed | tf_op | source)
XLA Modules:
  0.0 54.7 jit_solution(10776752283592603989)
XLA Ops:
  0.0 0.0 copy-start.9
  0.0 0.0 copy-start.11
  0.0 0.7 %copy-done.9 = f32[2048]{0:T(1024)S(1)} copy-done((f32[2048]{0:T(1024)S(1)}, f32[2048]{0:T(1024)}, u32[]{:S(2)}) %copy-start.9) | copy-done | bytes 8216
  0.7 0.0 copy-done.11
  0.7 0.0 copy-start
  0.7 1.2 %copy-done = bf16[1,256,2048]{2,1,0:T(8,128)(2,1)S(1)} copy-done((bf16[1,256,2048]{2,1,0:T(8,128)(2,1)S(1)}, bf16[1,256,2048]{2,1,0:T(8,128)(2,1)}, u32[]{:S(2)}) %copy-start) | copy-done | bytes 1048600
  1.9 0.0 copy-start.1
  1.9 1.2 %copy-done.1 = bf16[1,256,2048]{2,1,0:T(8,128)(2,1)S(1)} copy-done((bf16[1,256,2048]{2,1,0:T(8,128)(2,1)S(1)}, bf16[1,256,2048]{2,1,0:T(8,128)(2,1)}, u32[]{:S(2)}) %copy-start.1) | copy-done | bytes 1048600
  3.2 0.0 copy-start.2
  3.2 1.2 %copy-done.2 = bf16[2048,256]{1,0:T(8,128)(2,1)S(1)} copy-done((bf16[2048,256]{1,0:T(8,128)(2,1)S(1)}, bf16[2048,256]{1,0:T(8,128)(2,1)}, u32[]{:S(2)}) %copy-start.2) | copy-done | bytes 1048600
  4.4 0.0 copy-start.3
  4.4 1.2 %copy-done.3 = bf16[256,2048]{1,0:T(8,128)(2,1)S(1)} copy-done((bf16[256,2048]{1,0:T(8,128)(2,1)S(1)}, bf16[256,2048]{1,0:T(8,128)(2,1)}, u32[]{:S(2)}) %copy-start.3) | copy-done | bytes 1048600
  5.6 0.0 copy-start.4
  5.6 1.0 %copy-done.4 = bf16[512,512]{1,0:T(8,128)(2,1)S(1)} copy-done((bf16[512,512]{1,0:T(8,128)(2,1)S(1)}, bf16[512,512]{1,0:T(8,128)(2,1)}, u32[]{:S(2)}) %copy-start.4) | copy-done | bytes 524312
  6.6 0.0 copy-start.5
  6.6 1.0 %copy-done.5 = bf16[512,512]{1,0:T(8,128)(2,1)S(1)} copy-done((bf16[512,512]{1,0:T(8,128)(2,1)S(1)}, bf16[512,512]{1,0:T(8,128)(2,1)}, u32[]{:S(2)}) %copy-start.5) | copy-done | bytes 524312
  7.7 0.0 copy-start.6
  7.7 1.0 %copy-done.6 = bf16[512,512]{1,0:T(8,128)(2,1)S(1)} copy-done((bf16[512,512]{1,0:T(8,128)(2,1)S(1)}, bf16[512,512]{1,0:T(8,128)(2,1)}, u32[]{:S(2)}) %copy-start.6) | copy-done | bytes 524312
  8.7 0.0 copy-start.7
  8.7 0.9 %copy-done.7 = bf16[2048,64]{0,1:T(8,128)(2,1)S(1)} copy-done((bf16[2048,64]{0,1:T(8,128)(2,1)S(1)}, bf16[2048,64]{0,1:T(8,128)(2,1)}, u32[]{:S(2)}) %copy-start.7) | copy-done | bytes 262168
  9.7 0.0 copy-start.8
  9.7 0.9 %copy-done.8 = bf16[2048,64]{0,1:T(8,128)(2,1)S(1)} copy-done((bf16[2048,64]{0,1:T(8,128)(2,1)S(1)}, bf16[2048,64]{0,1:T(8,128)(2,1)}, u32[]{:S(2)}) %copy-start.8) | copy-done | bytes 262168
  10.6 0.0 copy-start.10
  10.6 0.7 %copy-done.10 = bf16[1,512]{1,0:T(2,128)(2,1)S(1)} copy-done((bf16[1,512]{1,0:T(2,128)(2,1)S(1)}, bf16[1,512]{1,0:T(2,128)(2,1)}, u32[]{:S(2)}) %copy-start.10) | copy-done | bytes 1048
  11.3 0.0 copy-start.12
  11.3 0.7 %copy-done.12 = f32[64]{0:T(128)S(1)} copy-done((f32[64]{0:T(128)S(1)}, f32[64]{0:T(128)}, u32[]{:S(2)}) %copy-start.12) | copy-done | bytes 280
  12.0 0.0 copy-start.13
  12.0 0.7 %copy-done.13 = f32[64]{0:T(128)S(1)} copy-done((f32[64]{0:T(128)S(1)}, f32[64]{0:T(128)}, u32[]{:S(2)}) %copy-start.13) | copy-done | bytes 280
  12.6 0.0 copy-start.14
  12.6 0.7 %copy-done.14 = f32[4]{0:T(128)S(1)} copy-done((f32[4]{0:T(128)S(1)}, f32[4]{0:T(128)}, u32[]{:S(2)}) %copy-start.14) | copy-done | bytes 40
  13.3 40.5 %shard_map.145 = bf16[1,256,2048]{2,1,0:T(8,128)(2,1)S(1)} custom-call(bf16[1,512]{1,0:T(2,128)(2,1)S(1)} %copy-done.10, bf16[512]{0:T(512)(128)(2,1)S(1)} %copy-done.11, f32[1,2048]{1,0:T(1,128)S(1)} %bitcast.7, f32[1,64]{1,0:T(1,128)S(1)} %bitcast.8, f32[1,64]{1,0:T(1,128)S(1)} %bitcast.9, f32[4]{0:T(128)S(1)} %copy-done.14, ...), custom_call_target="tpu_custom_call" | custom-call | tf_op jit(solution)/shard_map/pallas_call | solution.py:363
  53.7 1.0 %copy.17 = bf16[1,256,2048]{2,1,0:T(8,128)(2,1)} copy(bf16[1,256,2048]{2,1,0:T(8,128)(2,1)S(1)} %shard_map.145) | data formatting | bytes 2097152
Async XLA Ops:
  0.0 0.7 %copy-start.9 = (f32[2048]{0:T(1024)S(1)}, f32[2048]{0:T(1024)}, u32[]{:S(2)}) copy-start(f32[2048]{0:T(1024)} %param.22) | copy-start | bytes 24580
  0.0 0.7 %copy-start.11 = (bf16[512]{0:T(512)(128)(2,1)S(1)}, bf16[512]{0:T(512)(128)(2,1)}, u32[]{:S(2)}) copy-start(bf16[512]{0:T(512)(128)(2,1)} %code.1) | copy-start | bytes 3076
  0.7 1.2 %copy-start = (bf16[1,256,2048]{2,1,0:T(8,128)(2,1)S(1)}, bf16[1,256,2048]{2,1,0:T(8,128)(2,1)}, u32[]{:S(2)}) copy-start(bf16[1,256,2048]{2,1,0:T(8,128)(2,1)} %latent.1) | copy-start | bytes 3145732
  1.9 1.2 %copy-start.1 = (bf16[1,256,2048]{2,1,0:T(8,128)(2,1)S(1)}, bf16[1,256,2048]{2,1,0:T(8,128)(2,1)}, u32[]{:S(2)}) copy-start(bf16[1,256,2048]{2,1,0:T(8,128)(2,1)} %context.1) | copy-start | bytes 3145732
  3.2 1.2 %copy-start.2 = (bf16[2048,256]{1,0:T(8,128)(2,1)S(1)}, bf16[2048,256]{1,0:T(8,128)(2,1)}, u32[]{:S(2)}) copy-start(bf16[2048,256]{1,0:T(8,128)(2,1)} %wq.1) | copy-start | bytes 3145732
  4.4 1.2 %copy-start.3 = (bf16[256,2048]{1,0:T(8,128)(2,1)S(1)}, bf16[256,2048]{1,0:T(8,128)(2,1)}, u32[]{:S(2)}) copy-start(bf16[256,2048]{1,0:T(8,128)(2,1)} %wo.1) | copy-start | bytes 3145732
  5.6 1.0 %copy-start.4 = (bf16[512,512]{1,0:T(8,128)(2,1)S(1)}, bf16[512,512]{1,0:T(8,128)(2,1)}, u32[]{:S(2)}) copy-start(bf16[512,512]{1,0:T(8,128)(2,1)} %shift_w.1) | copy-start | bytes 1572868
  6.6 1.0 %copy-start.5 = (bf16[512,512]{1,0:T(8,128)(2,1)S(1)}, bf16[512,512]{1,0:T(8,128)(2,1)}, u32[]{:S(2)}) copy-start(bf16[512,512]{1,0:T(8,128)(2,1)} %scale_w.1) | copy-start | bytes 1572868
  7.7 1.0 %copy-start.6 = (bf16[512,512]{1,0:T(8,128)(2,1)S(1)}, bf16[512,512]{1,0:T(8,128)(2,1)}, u32[]{:S(2)}) copy-start(bf16[512,512]{1,0:T(8,128)(2,1)} %gate_w.1) | copy-start | bytes 1572868
  8.7 0.9 %copy-start.7 = (bf16[2048,64]{0,1:T(8,128)(2,1)S(1)}, bf16[2048,64]{0,1:T(8,128)(2,1)}, u32[]{:S(2)}) copy-start(bf16[2048,64]{0,1:T(8,128)(2,1)} %param.24) | copy-start | bytes 786436
  9.7 0.9 %copy-start.8 = (bf16[2048,64]{0,1:T(8,128)(2,1)S(1)}, bf16[2048,64]{0,1:T(8,128)(2,1)}, u32[]{:S(2)}) copy-start(bf16[2048,64]{0,1:T(8,128)(2,1)} %param.25) | copy-start | bytes 786436
  10.6 0.7 %copy-start.10 = (bf16[1,512]{1,0:T(2,128)(2,1)S(1)}, bf16[1,512]{1,0:T(2,128)(2,1)}, u32[]{:S(2)}) copy-start(bf16[1,512]{1,0:T(2,128)(2,1)} %condition.1) | copy-start | bytes 3076
  11.3 0.7 %copy-start.12 = (f32[64]{0:T(128)S(1)}, f32[64]{0:T(128)}, u32[]{:S(2)}) copy-start(f32[64]{0:T(128)} %param.27) | copy-start | bytes 772
  12.0 0.7 %copy-start.13 = (f32[64]{0:T(128)S(1)}, f32[64]{0:T(128)}, u32[]{:S(2)}) copy-start(f32[64]{0:T(128)} %param.28) | copy-start | bytes 772
  12.6 0.7 %copy-start.14 = (f32[4]{0:T(128)S(1)}, f32[4]{0:T(128)}, u32[]{:S(2)}) copy-start(f32[4]{0:T(128)} %bias_ref.1) | copy-start | bytes 52

commit v3 on v1

--- a/solution.py
+++ b/solution.py
@@ -86,7 +86,7 @@
 
     row8 = lax.broadcasted_iota(jnp.int32, (8, condition.shape[1]), 0)
     own_code = condition[...].astype(F32)
-    shared_code = code[...].astype(F32)
+    shared_code = code[...].astype(F32)[None]
     both = jnp.where(row8 == 0, own_code, jnp.where(row8 == 1, shared_code, 0.0))
     both = (both / (1.0 + jnp.exp(-both))).astype(BF16)
     pieces = []
@@ -227,11 +227,8 @@
                       + dots(p_l, values(kvbuf[block, crows:])))
 
     absorb(sp)
-    for d in near:
-        got_weights(d, 1)
-
-    @pl.loop(1, n_sp)
-    def _(s):
+
+    def forward(s):
         for part in range(2):
             @pl.when(sp - s >= 0)
             def _():
@@ -249,6 +246,7 @@
                 def _():
                     kv_copy(sp + s, sp - 1, 1, part).start()
 
+    def absorb_both(s):
         @pl.when(sp - s >= 0)
         def _():
             absorb(sp - s)
@@ -256,6 +254,18 @@
         @pl.when(sp + s < n_sp)
         def _():
             absorb(sp + s)
+
+    if n_sp > 1:
+        forward(1)
+    for d in near:
+        got_weights(d, 1)
+    if n_sp > 1:
+        absorb_both(1)
+
+    @pl.loop(2, n_sp)
+    def _(s):
+        forward(s)
+        absorb_both(s)
 
     if n_tp == 4:
         for part in range(2):
@@ -290,6 +300,7 @@
             remote(ref, ref, a_send.at[d, g], a_recv.at[d, g], tp=tp ^ d).wait_recv()
         return project(tp ^ d)
 
+    backs = []
     for d in range(n_tp):
         term = project(tp) if d == 0 else arrive(d)
         for t in range(n_tp):
@@ -302,8 +313,9 @@
             else:
                 gate = vec_t[t, 4:5, :]
                 out_v[:, part] = (lat[:, part].astype(F32) + gate * value).astype(BF16)
-    back = pltpu.make_async_copy(out_v, out.at[0], out_sem)
-    back.start()
+                back = pltpu.make_async_copy(out_v.at[:, part], out.at[0, :, part], out_sem.at[t])
+                back.start()
+                backs.append(back)
 
     for copy in waiting:
         copy.wait_send()
@@ -318,7 +330,8 @@
             @pl.when((b >= sp) & (sp > 0))
             def _():
                 kv_copy(b, sp, 1, part).wait_send()
-    back.wait()
+    for back in backs:
+        back.wait()
 
 
 def on_device(
@@ -358,7 +371,7 @@
         pltpu.VMEM((rows, hd), F32),
         pltpu.VMEM((rows, 1), F32),
         pltpu.VMEM((rows, width), BF16),
-        dma((9,)), dma,
+        dma((9,)), dma((n_tp,)),
         dma((n_sp,)), dma((n_sp,)), dma((n_tp,)), dma((n_tp,)),
         dma((2, 2, n_sp)), dma((2, n_sp)),
         dma((n_tp, 2)), dma((n_tp, 2)), dma((n_tp, 2, n_dp)), dma((n_tp, 2, n_dp)),
@@ -373,7 +386,7 @@
         compiler_params=pltpu.CompilerParams(
             collective_id=0, has_side_effects=True, vmem_limit_bytes=60 * 1024 * 1024),
     )(
-        condition, context_code[None], norm_gain[None], query_gain[None], key_gain[None],
+        condition, context_code, norm_gain[None], query_gain[None], key_gain[None],
         context_bias, latent, context, shift_weight, scale_weight, gate_weight, query_weight,
         key_weight.T, value_weight.T, output_weight,
     )

time: 45.3 us -> 43.7 us (0.965)
  local copies, waits for them, and re-layouts: 3.56 us -> 2.3 us
    unnamed x3 -> x1, local copies, waits for them, and re-layouts: 2.98 us -> 2.3 us
    broadcast_in_dim x1 -> x0, local copies, waits for them, and re-layouts: 0.58 us -> none  [on_device(): context_code[None]]
where the time goes in v3:
time: 43.7 us; the launch traced here: 43.5 us
  Pallas kernels  41.2 us (94%)
  local copies, waits for them, and re-layouts  2.3 us (5%)
    pallas_call x1, Pallas kernels, on_device(): pl.pallas_call(functools.partial(kernel, sizes), out_shape=jax.ShapeDtype...  41.2 us
    unnamed x1, local copies, waits for them, and re-layouts  2.3 us

profile of v3, /device:TPU:0, one launch (start us, length us, event | category | flops | bytes accessed | tf_op | source)
XLA Modules:
  0.0 43.5 jit_solution(16742840844223136857)
XLA Ops:
  0.0 41.2 %shard_map.145 = bf16[1,256,2048]{2,1,0:T(8,128)(2,1)} custom-call(bf16[1,512]{1,0:T(2,128)(2,1)} %condition.1, bf16[512]{0:T(512)(128)(2,1)} %code.1, f32[1,2048]{1,0:T(1,128)} %bitcast.7, f32[1,64]{1,0:T(1,128)} %bitcast.8, f32[1,64]{1,0:T(1,128)} %bitcast.9, f32[4]{0:T(128)} %bias_ref.1, bf16[1,256,2048]{2,1,0:T(8,128)(2,1)} %latent.1, ...), custom_call_target="tpu_custom_call" | custom-call | tf_op jit(solution)/shard_map/pallas_call | solution.py:380
  41.2 2.3 %copy.17 = bf16[1,256,2048]{2,1,0:T(8,128)(2,1)} copy(bf16[1,256,2048]{2,1,0:T(8,128)(2,1)} %shard_map.145) | data formatting | bytes 2097152

commit v4 on v3

--- a/solution.py
+++ b/solution.py
@@ -205,7 +205,7 @@
         got_weights(d, 0)
 
     def absorb(block):
-        @pl.loop(0, heads)
+        @pl.loop(0, heads, unroll=2)
         def _(h):
             bias = bias_ref[h]
             query = q_s[h]

time: 43.7 us -> 42.1 us (0.963)
  Pallas kernels: 41.2 us -> 39.6 us
    pallas_call x1, Pallas kernels: 41.2 us -> 39.6 us  [on_device(): pl.pallas_call(functools.partial(kernel, sizes), out_shape=jax.ShapeDtype...]
where the time goes in v4:
time: 42.1 us; the launch traced here: 41.9 us
  Pallas kernels  39.6 us (94%)
  local copies, waits for them, and re-layouts  2.3 us (5%)
    pallas_call x1, Pallas kernels, on_device(): pl.pallas_call(functools.partial(kernel, sizes), out_shape=jax.ShapeDtype...  39.6 us
    unnamed x1, local copies, waits for them, and re-layouts  2.3 us

profile of v4, /device:TPU:0, one launch (start us, length us, event | category | flops | bytes accessed | tf_op | source)
XLA Modules:
  0.0 41.9 jit_solution(8946033876914509770)
XLA Ops:
  0.0 39.6 %shard_map.145 = bf16[1,256,2048]{2,1,0:T(8,128)(2,1)} custom-call(bf16[1,512]{1,0:T(2,128)(2,1)} %condition.1, bf16[512]{0:T(512)(128)(2,1)} %code.1, f32[1,2048]{1,0:T(1,128)} %bitcast.7, f32[1,64]{1,0:T(1,128)} %bitcast.8, f32[1,64]{1,0:T(1,128)} %bitcast.9, f32[4]{0:T(128)} %bias_ref.1, bf16[1,256,2048]{2,1,0:T(8,128)(2,1)} %latent.1, ...), custom_call_target="tpu_custom_call" | custom-call | tf_op jit(solution)/shard_map/pallas_call | solution.py:380
  39.6 2.3 %copy.17 = bf16[1,256,2048]{2,1,0:T(8,128)(2,1)} copy(bf16[1,256,2048]{2,1,0:T(8,128)(2,1)} %shard_map.145) | data formatting | bytes 2097152
